TPU v7x, 32 devices: a whole 2x2x4 slice. The times are simulated.
32 devices in a mesh: grp: 2 (over y), sp: 4 (over z), tp: 4 (over x, core).
Axes of the slice: x: 2, y: 2, z: 4, core: 2. Of those that a mesh axis runs over, the one named last changes fastest.
Arguments:
- source: bfloat16 [4096, 2048], P(('grp', 'sp', 'tp')), parts along dimension 0, may hold values from -8 to 8
- target: bfloat16 [1024, 2048], P(('grp', 'sp', 'tp')), parts along dimension 0, may hold values from -8 to 8
- source_gain: float32 [2048], replicated, may hold values from 0.1 to 1.9
- attend_gain: float32 [2, 2048], replicated, may hold values from 0.1 to 1.9
- query_weight: bfloat16 [2, 2048, 2048], P(None, None, 'tp'), may hold values from -4 to 4
- key_weight: bfloat16 [2, 2048, 2048], P(None, None, 'tp'), may hold values from -4 to 4
- value_weight: bfloat16 [2, 2048, 2048], P(None, None, 'tp'), may hold values from -0.125 to 0.125
- out_weight: bfloat16 [2, 2048, 2048], P(None, 'tp'), may hold values from -3 to 3
- mixer_gain: float32 [2048], replicated, may hold values from 0.1 to 1.9
- gate_weight: bfloat16 [2048, 2816], P(None, 'tp'), may hold values from -0.125 to 0.125
- up_weight: bfloat16 [2048, 2816], P(None, 'tp'), may hold values from -0.125 to 0.125
- gate_taps: float32 [3, 2816], P(None, 'tp'), may hold values from -3 to 3
- up_taps: float32 [3, 2816], P(None, 'tp'), may hold values from -3 to 3
- down_weight: bfloat16 [2816, 2048], P('tp'), may hold values from -0.109375 to 0.109375
- final_gain: float32 [2048], replicated, may hold values from 0.1 to 1.9
Outputs:
- result: bfloat16 [1024, 2048], P(('grp', 'sp', 'tp')), parts along dimension 0
There are 2 independent parts, one for each index of `grp`. A program takes and returns all parts, laid end to end along the dimension named above; an argument that names none is the same for every part. Nothing has to cross between parts.
All inputs are finite; a program needn't handle non-finite values.
Results may differ from a plain program's by a relative error of at most 0.04.
Values may be sent and summed in bfloat16 or wider, within the bound.
A program may use at most 128 MiB of HBM per device.

v0:
```python
import jax
import jax.numpy as jnp
from jax import lax
from jax.sharding import PartitionSpec as P

HD = 256
EPS = 1e-06


def shifted(value, axis, steps):
    count = lax.axis_size(axis)
    first, last = (max(0, -steps), min(count, count - steps))
    return lax.ppermute(value, axis, [(source, source + steps) for source in range(first, last)])


def normed_rows(rows, gain):
    wide = rows.astype(jnp.float32)
    return wide * lax.rsqrt(jnp.mean(wide * wide, axis=-1, keepdims=True) + EPS) * gain


def attend_layer(residual, key_rows, value_rows, gain, w_query, w_out):
    width = w_query.shape[1]
    heads_here = width // HD
    head_scale = HD ** (-0.5)
    normed = normed_rows(residual, gain).astype(jnp.bfloat16)
    query_block = jnp.dot(
        lax.all_gather(normed, "tp", axis=0, tiled=True),
        w_query,
        preferred_element_type=jnp.float32,
    ).astype(jnp.bfloat16)
    row_count = query_block.shape[0]
    key_heads = key_rows.reshape(-1, heads_here, HD)
    value_heads = value_rows.reshape(-1, heads_here, HD)
    every_query = lax.all_gather(query_block, "sp", axis=0, tiled=True)
    every_heads = every_query.reshape(-1, heads_here, HD)
    scores = (
        jnp.einsum("thd,shd->hts", every_heads, key_heads, preferred_element_type=jnp.float32)
        * head_scale
    )
    highest = lax.pmax(jnp.max(scores, axis=-1), "sp")
    raised = jnp.exp(scores - highest[:, :, None])
    weighted = jnp.einsum(
        "hts,shd->thd", raised.astype(jnp.bfloat16), value_heads, preferred_element_type=jnp.float32
    )
    row_totals = jnp.sum(raised, axis=-1).T
    own_sums, own_totals = (
        lax.psum_scatter(
            weighted.astype(jnp.bfloat16), "sp", scatter_dimension=0, tiled=True
        ).astype(jnp.float32),
        lax.psum_scatter(
            row_totals.astype(jnp.bfloat16), "sp", scatter_dimension=0, tiled=True
        ).astype(jnp.float32),
    )
    attended = (own_sums / own_totals[:, :, None]).reshape(row_count, width).astype(jnp.bfloat16)
    return lax.psum_scatter(
        jnp.dot(attended, w_out, preferred_element_type=jnp.float32).astype(jnp.bfloat16),
        "tp",
        scatter_dimension=0,
        tiled=True,
    ).astype(jnp.float32)


def body(
    source,
    target,
    source_gain,
    attend_gain,
    query_weight,
    key_weight,
    value_weight,
    out_weight,
    mixer_gain,
    gate_weight,
    up_weight,
    gate_taps,
    up_taps,
    down_weight,
    final_gain,
):
    width = query_weight.shape[2]
    source_normed = normed_rows(source, source_gain).astype(jnp.bfloat16)
    joined_weights = jnp.concatenate(
        [key_weight[0], value_weight[0], key_weight[1], value_weight[1]], axis=1
    )
    projected = jnp.dot(
        lax.all_gather(source_normed, "tp", axis=0, tiled=True),
        joined_weights,
        preferred_element_type=jnp.float32,
    ).astype(jnp.bfloat16)
    residual = target.astype(jnp.float32)
    for layer_number in range(2):
        key_rows = projected[:, 2 * layer_number * width : (2 * layer_number + 1) * width]
        value_rows = projected[:, (2 * layer_number + 1) * width : (2 * layer_number + 2) * width]
        residual = residual + attend_layer(
            residual,
            key_rows,
            value_rows,
            attend_gain[layer_number],
            query_weight[layer_number],
            out_weight[layer_number],
        )
    mixed = normed_rows(residual, mixer_gain).astype(jnp.bfloat16)
    portion = lax.all_gather(mixed, "tp", axis=0, tiled=True)
    gate_part = jnp.dot(portion, gate_weight, preferred_element_type=jnp.float32)
    up_part = jnp.dot(portion, up_weight, preferred_element_type=jnp.float32)
    lifted = jnp.concatenate([gate_part, up_part], axis=1).astype(jnp.bfloat16)
    earlier = shifted(lifted[-2:], "sp", 1)
    padded = jnp.concatenate([earlier, lifted], axis=0).astype(jnp.float32)
    all_taps = jnp.concatenate([gate_taps, up_taps], axis=1)
    convolved = all_taps[0] * padded[:-2] + all_taps[1] * padded[1:-1] + all_taps[2] * padded[2:]
    inner_units = gate_weight.shape[1]
    hidden = (jax.nn.silu(convolved[:, :inner_units]) * convolved[:, inner_units:]).astype(
        jnp.bfloat16
    )
    residual = residual + lax.psum_scatter(
        jnp.dot(hidden, down_weight, preferred_element_type=jnp.float32).astype(jnp.bfloat16),
        "tp",
        scatter_dimension=0,
        tiled=True,
    ).astype(jnp.float32)
    return normed_rows(residual, final_gain).astype(jnp.bfloat16)


def solution(mesh):
    placed = (
        P(("grp", "sp", "tp"), None),
        P(("grp", "sp", "tp"), None),
        P(),
        P(),
        P(None, None, "tp"),
        P(None, None, "tp"),
        P(None, None, "tp"),
        P(None, "tp", None),
        P(),
        P(None, "tp"),
        P(None, "tp"),
        P(None, "tp"),
        P(None, "tp"),
        P("tp", None),
        P(),
    )
    return jax.shard_map(
        body, mesh=mesh, in_specs=placed, out_specs=P(("grp", "sp", "tp"), None), check_vma=False
    )
```

profile of v0, /device:TPU:0, one launch (start us, length us, event | category | flops | bytes accessed | tf_op | source)
XLA Modules:
  0.0 301.9 jit_solution(114304977294703288)
XLA Ops:
  6.5 1.4 fusion.31
  7.9 2.1 fusion.33
  10.0 0.0 all-gather.2.cloned.1.call-update
  10.0 0.0 reduce-scatter.24.cloned.1.call-start
  10.1 0.1 fusion.53
  10.3 0.1 fusion.55
  10.4 8.8 %all_gather.19 = bf16[128,2048]{1,0:T(8,128)(2,1)S(1)} all-gather(bf16[32,2048]{1,0:T(8,128)(2,1)S(1)} %fusion.55), channel_id=1, replica_groups=mesh['grp'=2,'sp'=4,'tp'=4] {'tp'}, dimensions={0}, use_global_device_ids=true | all-gather | bytes 655360 | tf_op jit(solution)/shard_map/all_gather | solution.py:27
  19.2 2.2 fusion.25
  21.3 16.3 %all_gather.20 = bf16[512,512]{1,0:T(8,128)(2,1)S(1)} all-gather(bf16[128,512]{1,0:T(8,128)(2,1)S(1)} %fusion.25), channel_id=1, replica_groups=mesh['grp'=2,'sp'=4,'tp'=4] {'sp'}, dimensions={0}, use_global_device_ids=true | all-gather | bytes 655360 | tf_op jit(solution)/shard_map/all_gather | solution.py:34
  37.7 4.9 %slice_bitcast_fusion.2 = (bf16[2048,512]{1,0:T(8,128)(2,1)}, bf16[2048,512]{1,0:T(8,128)(2,1)}, bf16[2048,512]{1,0:T(8,128)(2,1)}, bf16[2048,512]{1,0:T(8,128)(2,1)}) fusion(bf16[2,2048,512]{2,1,0:T(8,128)(2,1)S(1)} %copy-done.3, bf16[2,2048,512]{2,1,0:T(8,128)(2,1)} %param.20), kind=kLoop, calls=%fused_computation.26 | loop fusion | bytes 16777216 | tf_op jit(solution)/shard_map/squeeze | solution.py:83
  42.6 8.9 %fusion.8 = bf16[512,2048]{1,0:T(8,128)(2,1)S(1)} fusion(bf16[512,2048]{1,0:T(8,128)(2,1)} %all-gather.2.cloned.1.call-done, bf16[2048,512]{1,0:T(8,128)(2,1)} %get-tuple-element.11, bf16[2048,512]{1,0:T(8,128)(2,1)} %get-tuple-element.22, bf16[2048,512]{1,0:T(8,128)(2,1)} %get-tuple-element.10, bf16[2048,512]{1,0:T(8,128)(2,1)} %get-tuple-element.23), kind=kOutput, calls=%fused_computation.8 | convolution fusion | flops 4329570304 | bytes 12582912 | tf_op jit(solution)/shard_map/dot_general | solution.py:85
  51.5 1.2 fusion.63
  52.7 1.8 multiply_reduce_fusion.1
  54.5 12.1 %pmax.14 = f32[2,512]{1,0:T(2,128)S(1)} all-reduce(f32[2,512]{1,0:T(2,128)S(1)} %get-tuple-element.18), channel_id=1, replica_groups=mesh['grp'=2,'sp'=4,'tp'=4] {'sp'}, use_global_device_ids=true, to_apply=%region_3.0 | all-reduce | flops 1024 | bytes 8192 | tf_op jit(solution)/shard_map/pmax | solution.py:40
  66.6 1.3 copy.34
  67.9 2.0 fusion.21
  69.8 0.8 copy.38
  70.7 0.0 reduce-scatter.22.cloned.1.call-start
  70.7 2.9 convolution_convert_fusion.4
  73.6 2.1 copy.44
  75.7 0.0 reduce-scatter.16.cloned.1.call-start
  75.8 12.4 %reduce-scatter.24.cloned.1.call-done = bf16[128,2]{1,0:T(8,128)(2,1)} async-done(((bf16[512,2]{1,0:T(8,128)(2,1)}), bf16[128,2]{1,0:T(8,128)(2,1)}) %reduce-scatter.24.cloned.1.call-update) | async-done | bytes 528
  88.1 0.8 copy.39
  89.0 21.5 %reduce-scatter.22.cloned.1.call-done = bf16[128,512]{1,0:T(8,128)(2,1)} async-done(((bf16[512,512]{1,0:T(8,128)(2,1)}), bf16[128,512]{1,0:T(8,128)(2,1)}) %reduce-scatter.22.cloned.1.call-update) | async-done | bytes 131088
  110.4 1.0 copy.45
  111.5 2.9 convolution_convert_fusion.2
  114.4 0.0 reduce-scatter.28.cloned.1.call-start
  114.4 1.3 copy.35
  115.7 18.8 %reduce-scatter.16.cloned.1.call-done = bf16[32,2048]{1,0:T(8,128)(2,1)} async-done(((bf16[128,2048]{1,0:T(8,128)(2,1)}), bf16[32,2048]{1,0:T(8,128)(2,1)}) %reduce-scatter.16.cloned.1.call-update) | async-done | bytes 131088 | tf_op jit(solution)/shard_map/reduce_scatter | solution.py:55
  134.4 1.1 multiply_reduce_fusion.4
  135.5 1.0 multiply_convert_fusion.2
  136.5 6.6 %all_gather.21 = bf16[128,2048]{1,0:T(8,128)(2,1)S(1)} all-gather(bf16[32,2048]{1,0:T(8,128)(2,1)S(1)} %multiply_convert_fusion.2), channel_id=1, replica_groups=mesh['grp'=2,'sp'=4,'tp'=4] {'tp'}, dimensions={0}, use_global_device_ids=true | all-gather | bytes 655360 | tf_op jit(solution)/shard_map/all_gather | solution.py:27
  143.1 2.1 fusion.28
  145.2 16.1 %all_gather.22 = bf16[512,512]{1,0:T(8,128)(2,1)S(1)} all-gather(bf16[128,512]{1,0:T(8,128)(2,1)S(1)} %fusion.28), channel_id=1, replica_groups=mesh['grp'=2,'sp'=4,'tp'=4] {'sp'}, dimensions={0}, use_global_device_ids=true | all-gather | bytes 655360 | tf_op jit(solution)/shard_map/all_gather | solution.py:34
  161.3 1.8 multiply_reduce_fusion
  163.1 12.2 %pmax.15 = f32[2,512]{1,0:T(2,128)S(1)} all-reduce(f32[2,512]{1,0:T(2,128)S(1)} %get-tuple-element.20), channel_id=1, replica_groups=mesh['grp'=2,'sp'=4,'tp'=4] {'sp'}, use_global_device_ids=true, to_apply=%region_10.0 | all-reduce | flops 1024 | bytes 8192 | tf_op jit(solution)/shard_map/pmax | solution.py:40
  175.3 2.0 fusion.23
  177.3 0.8 copy.42
  178.1 0.0 reduce-scatter.26.cloned.1.call-start
  178.2 2.9 convolution_convert_fusion.3
  181.1 2.1 copy.46
  183.2 0.0 reduce-scatter.18.cloned.1.call-start
  183.2 12.2 %reduce-scatter.28.cloned.1.call-done = bf16[128,2]{1,0:T(8,128)(2,1)} async-done(((bf16[512,2]{1,0:T(8,128)(2,1)}), bf16[128,2]{1,0:T(8,128)(2,1)}) %reduce-scatter.28.cloned.1.call-update) | async-done | bytes 528
  195.4 0.8 copy.43
  196.3 21.4 %reduce-scatter.26.cloned.1.call-done = bf16[128,512]{1,0:T(8,128)(2,1)} async-done(((bf16[512,512]{1,0:T(8,128)(2,1)}), bf16[128,512]{1,0:T(8,128)(2,1)}) %reduce-scatter.26.cloned.1.call-update) | async-done | bytes 131088
  217.6 1.0 copy.47
  218.7 2.9 convolution_convert_fusion.1
  221.6 0.0 reduce-scatter.20.cloned.1.call-start
  221.6 20.0 %reduce-scatter.18.cloned.1.call-done = bf16[32,2048]{1,0:T(8,128)(2,1)} async-done(((bf16[128,2048]{1,0:T(8,128)(2,1)}), bf16[32,2048]{1,0:T(8,128)(2,1)}) %reduce-scatter.18.cloned.1.call-update) | async-done | bytes 131088 | tf_op jit(solution)/shard_map/reduce_scatter | solution.py:55
  241.6 1.1 multiply_reduce_fusion.3
  242.7 1.0 multiply_convert_fusion.1
  243.7 6.9 %all_gather.23 = bf16[128,2048]{1,0:T(8,128)(2,1)S(1)} all-gather(bf16[32,2048]{1,0:T(8,128)(2,1)S(1)} %multiply_convert_fusion.1), channel_id=1, replica_groups=mesh['grp'=2,'sp'=4,'tp'=4] {'tp'}, dimensions={0}, use_global_device_ids=true | all-gather | bytes 655360 | tf_op jit(solution)/shard_map/all_gather | solution.py:103
  250.6 2.7 convolution_convert_fusion.5
  253.4 0.9 convolution_convert_fusion.6
  254.3 0.2 pad_maximum_fusion
  254.5 3.4 %collective-permute-start = (bf16[2,1408]{0,1:T(8,128)(2,1)S(1)}, bf16[2,1408]{0,1:T(8,128)(2,1)S(1)}, u32[]{:S(2)}, u32[]{:S(2)}) collective-permute-start(bf16[2,1408]{0,1:T(8,128)(2,1)S(1)} %pad_maximum_fusion), channel_id=1, source_target_pairs={{0,4},{4,8},{8,12},{1,5},{5,9},{9,13},{2,6},{6,10},{10,14},{3,7},{... | collective-permute-start | bytes 16904 | tf_op jit(solution)/shard_map/ppermute | solution.py:13
  257.9 0.1 maximum_reduce_fusion.1
  258.0 8.0 %collective-permute-done = bf16[2,1408]{0,1:T(8,128)(2,1)S(1)} collective-permute-done((bf16[2,1408]{0,1:T(8,128)(2,1)S(1)}, bf16[2,1408]{0,1:T(8,128)(2,1)S(1)}, u32[]{:S(2)}, u32[]{:S(2)}) %collective-permute-start) | collective-permute-done | bytes 5664 | tf_op jit(solution)/shard_map/ppermute | solution.py:13
  266.1 0.3 maximum_convert_fusion
  266.3 1.1 fusion.40
  267.5 1.4 convolution_convert_fusion
  269.0 23.3 %reduce-scatter.20.cloned.1.call-done = bf16[32,2048]{1,0:T(8,128)(2,1)} async-done(((bf16[128,2048]{1,0:T(8,128)(2,1)}), bf16[32,2048]{1,0:T(8,128)(2,1)}) %reduce-scatter.20.cloned.1.call-update) | async-done | bytes 131088 | tf_op jit(solution)/shard_map/reduce_scatter | solution.py:115
  292.3 1.1 multiply_reduce_fusion.2
  293.4 1.7 multiply_convert_fusion
  (43 shorter events, 0.3 us)
Async XLA Ops:
  6.5 261.0 %copy-start = (bf16[704,2048]{1,0:T(8,128)(2,1)S(1)}, bf16[704,2048]{1,0:T(8,128)(2,1)}, u32[]{:S(2)}) copy-start(bf16[704,2048]{1,0:T(8,128)(2,1)} %param.28) | copy-start | bytes 8650756
  6.5 3.5 %copy-start.1 = (bf16[32,2048]{1,0:T(8,128)(2,1)S(1)}, bf16[32,2048]{1,0:T(8,128)(2,1)}, u32[]{:S(2)}) copy-start(bf16[32,2048]{1,0:T(8,128)(2,1)} %param.16) | copy-start | bytes 393220
  6.5 3.7 %copy-start.7 = (f32[2,2048]{1,0:T(2,128)S(1)}, f32[2,2048]{1,0:T(2,128)}, u32[]{:S(2)}) copy-start(f32[2,2048]{1,0:T(2,128)} %param.18) | copy-start | bytes 49156
  6.5 36.1 %all-gather.2.cloned.1.call-start = ((), (), s32[]{:S(2)}) async-start(), calls=%async_computation.7 | async-start | bytes 2621440 | tf_op jit(solution)/shard_map/all_gather | solution.py:86
  10.0 78.1 %reduce-scatter.24.cloned.1.call-start = ((), (), s32[]{:S(2)}) async-start(), calls=%async_computation.12 | async-start | bytes 163840
  10.4 27.3 %copy-start.3 = (bf16[2,2048,512]{2,1,0:T(8,128)(2,1)S(1)}, bf16[2,2048,512]{2,1,0:T(8,128)(2,1)}, u32[]{:S(2)}) copy-start(bf16[2,2048,512]{2,1,0:T(8,128)(2,1)} %param.21) | copy-start | bytes 12582916
  70.7 39.7 %reduce-scatter.22.cloned.1.call-start = ((), (), s32[]{:S(2)}) async-start(), calls=%async_computation.11 | async-start | bytes 655360
  75.7 58.7 %reduce-scatter.16.cloned.1.call-start = ((), (), s32[]{:S(2)}) async-start(), calls=%async_computation.8 | async-start | bytes 655360 | tf_op jit(solution)/shard_map/reduce_scatter | solution.py:55
  114.4 81.1 %reduce-scatter.28.cloned.1.call-start = ((), (), s32[]{:S(2)}) async-start(), calls=%async_computation.14 | async-start | bytes 163840
  143.1 18.2 %copy-start.6 = (bf16[512,512]{1,0:T(8,128)(2,1)S(1)}, bf16[512,512]{1,0:T(8,128)(2,1)}, u32[]{:S(2)}) copy-start(bf16[512,512]{1,0:T(8,128)(2,1)} %get-tuple-element.13) | copy-start | bytes 1572868
  178.1 39.5 %reduce-scatter.26.cloned.1.call-start = ((), (), s32[]{:S(2)}) async-start(), calls=%async_computation.13 | async-start | bytes 655360
  183.1 58.5 %copy-start.2 = (bf16[32,2048]{1,0:T(8,128)(2,1)S(1)}, bf16[32,2048]{1,0:T(8,128)(2,1)}, u32[]{:S(2)}) copy-start(bf16[32,2048]{1,0:T(8,128)(2,1)} %reduce-scatter.16.cloned.1.call-done) | copy-start | bytes 393220
  183.2 58.4 %reduce-scatter.18.cloned.1.call-start = ((), (), s32[]{:S(2)}) async-start(), calls=%async_computation.9 | async-start | bytes 655360 | tf_op jit(solution)/shard_map/reduce_scatter | solution.py:55
  196.3 46.4 %copy-start.10 = (f32[2048]{0:T(1024)S(1)}, f32[2048]{0:T(1024)}, u32[]{:S(2)}) copy-start(f32[2048]{0:T(1024)} %param.23) | copy-start | bytes 24580
  221.6 70.7 %reduce-scatter.20.cloned.1.call-start = ((), (), s32[]{:S(2)}) async-start(), calls=%async_computation.10 | async-start | bytes 655360 | tf_op jit(solution)/shard_map/reduce_scatter | solution.py:115
  243.7 9.7 %copy-start.4 = (bf16[2048,704]{0,1:T(8,128)(2,1)S(1)}, bf16[2048,704]{0,1:T(8,128)(2,1)}, u32[]{:S(2)}) copy-start(bf16[2048,704]{0,1:T(8,128)(2,1)} %param.24) | copy-start | bytes 8650756
  253.4 4.5 %copy-start.8 = (f32[3,704]{1,0:T(4,128)S(1)}, f32[3,704]{1,0:T(4,128)}, u32[]{:S(2)}) copy-start(f32[3,704]{1,0:T(4,128)} %param.27) | copy-start | bytes 25348
  253.4 4.5 %copy-start.9 = (f32[3,704]{1,0:T(4,128)S(1)}, f32[3,704]{1,0:T(4,128)}, u32[]{:S(2)}) copy-start(f32[3,704]{1,0:T(4,128)} %param.26) | copy-start | bytes 25348
  254.5 11.6 %collective-permute-start = (bf16[2,1408]{0,1:T(8,128)(2,1)S(1)}, bf16[2,1408]{0,1:T(8,128)(2,1)S(1)}, u32[]{:S(2)}, u32[]{:S(2)}) collective-permute-start(bf16[2,1408]{0,1:T(8,128)(2,1)S(1)} %pad_maximum_fusion), channel_id=1, source_target_pairs={{0,4},{4,8},{8,12},{1,5},{5,9},{9,13},{2,6},{6,10},{10,14},{3,7},{... | collective-permute-start | bytes 16904 | tf_op jit(solution)/shard_map/ppermute | solution.py:13
  267.5 24.8 %copy-start.5 = (bf16[32,2048]{1,0:T(8,128)(2,1)S(1)}, bf16[32,2048]{1,0:T(8,128)(2,1)}, u32[]{:S(2)}) copy-start(bf16[32,2048]{1,0:T(8,128)(2,1)} %reduce-scatter.18.cloned.1.call-done) | copy-start | bytes 393220
  267.5 25.9 %copy-start.11 = (f32[2048]{0:T(1024)S(1)}, f32[2048]{0:T(1024)}, u32[]{:S(2)}) copy-start(f32[2048]{0:T(1024)} %param.29) | copy-start | bytes 24580
Sparse Core Ops, SparseCore 0:
  10.1 25.2 all-gather.1
  70.8 17.2 reduce-scatter.23
  90.4 19.9 reduce-scatter.21
  114.5 19.9 reduce-scatter.15
  178.2 17.1 reduce-scatter.27
  197.6 20.0 reduce-scatter.25
  221.7 19.8 reduce-scatter.17
  269.1 23.1 reduce-scatter.19
where the time goes:
time: 303 us; the launch traced here: 302 us
  waiting for transfers between devices  138 us (46%)
  blocking collectives  79 us (26%)
  matrix products  33.5 us (11%)
  local copies, waits for them, and re-layouts  18.1 us (6%)
  other arithmetic  16.3 us (5%)
  between operations  13.8 us (5%)
  starting transfers between devices  3.69 us (1%)
    unnamed x12, waiting for transfers between devices  67.5 us
    reduce_scatter x2, waiting for transfers between devices, attend_layer(): lax.psum_scatter(jnp.dot(attended, w_out, preferred_element_type=jnp.floa...  38.7 us
    all_gather x2, blocking collectives, attend_layer(): every_query = lax.all_gather(query_block, 'sp', axis=0, tiled=True)  32.4 us
    pmax x2, blocking collectives, attend_layer(): highest = lax.pmax(jnp.max(scores, axis=-1), 'sp')  24.3 us
    reduce_scatter x1, waiting for transfers between devices, body(): lax.psum_scatter(jnp.dot(hidden, down_weight, preferred_element_type=jnp....  23.3 us
    all_gather x2, blocking collectives, attend_layer(): lax.all_gather(normed, 'tp', axis=0, tiled=True)  15.4 us
    unnamed x32, local copies, waits for them, and re-layouts  9.48 us
    dot_general x1, matrix products, body(): jnp.dot(lax.all_gather(source_normed, 'tp', axis=0, tiled=True), joined_w...  8.9 us
  transfers between devices with their start and end apart: 9, of which 8 were waited for; matrix products, arithmetic and copies ran while one was open for 7% of the time, Pallas kernels for 0%

commit v1 on v0

--- a/solution.py
+++ b/solution.py
@@ -31,7 +31,13 @@
     row_count = query_block.shape[0]
     key_heads = key_rows.reshape(-1, heads_here, HD)
     value_heads = value_rows.reshape(-1, heads_here, HD)
-    every_query = lax.all_gather(query_block, "sp", axis=0, tiled=True)
+    size = lax.axis_size("sp")
+    moving, shards = (query_block, [query_block])
+    for _ in range(size - 1):
+        moving = lax.ppermute(moving, "sp", [(i, (i + 1) % size) for i in range(size)])
+        shards.insert(0, moving)
+    line = jnp.concatenate(shards, axis=0)
+    every_query = jnp.roll(line, (lax.axis_index("sp") + 1) * query_block.shape[0], axis=0)
     every_heads = every_query.reshape(-1, heads_here, HD)
     scores = (
         jnp.einsum("thd,shd->hts", every_heads, key_heads, preferred_element_type=jnp.float32)

time: 303 us -> 316 us (1.043)
  blocking collectives: 79 us -> 40.8 us
  waiting for transfers between devices: 138 us -> 174 us
  local copies, waits for them, and re-layouts: 18.1 us -> 23.5 us
  other arithmetic: 16.3 us -> 20.8 us
    ppermute x0 -> x6, waiting for transfers between devices: none -> 33.6 us  [attend_layer(): lax.ppermute(moving, 'sp', [(i, (i + 1) % size) for i in range(size)])]
    all_gather x2 -> x0, blocking collectives: 32.4 us -> none  [attend_layer(): every_query = lax.all_gather(query_block, 'sp', axis=0, tiled=True)]
    pmax x2, blocking collectives: 24.3 us -> 18.7 us  [attend_layer(): highest = lax.pmax(jnp.max(scores, axis=-1), 'sp')]
    concatenate x0 -> x2, other arithmetic: none -> 4.46 us  [attend_layer(): jnp.roll(line, (lax.axis_index('sp') + 1) * query_block.shape[0], axis=0)]
    unnamed x32 -> x48, local copies, waits for them, and re-layouts: 9.48 us -> 12.1 us
  transfers between devices with their start and end apart: 9 -> 15, of which waited for: 8 -> 14; matrix products, arithmetic and copies ran while one was open for 7% -> 7% of each run, Pallas kernels for 0% -> 0%
where the time goes in v1:
time: 316 us; the launch traced here: 315 us
  waiting for transfers between devices  174 us (55%)
  blocking collectives  40.8 us (13%)
  matrix products  35.6 us (11%)
  local copies, waits for them, and re-layouts  23.5 us (7%)
  other arithmetic  20.8 us (7%)
  between operations  13.8 us (4%)
  starting transfers between devices  6.82 us (2%)
    unnamed x12, waiting for transfers between devices  69.1 us
    reduce_scatter x2, waiting for transfers between devices, attend_layer(): lax.psum_scatter(jnp.dot(attended, w_out, preferred_element_type=jnp.floa...  40 us
    ppermute x6, waiting for transfers between devices, attend_layer(): lax.ppermute(moving, 'sp', [(i, (i + 1) % size) for i in range(size)])  33.6 us
    reduce_scatter x1, waiting for transfers between devices, body(): lax.psum_scatter(jnp.dot(hidden, down_weight, preferred_element_type=jnp....  23.4 us
    pmax x2, blocking collectives, attend_layer(): highest = lax.pmax(jnp.max(scores, axis=-1), 'sp')  18.7 us
    all_gather x2, blocking collectives, attend_layer(): lax.all_gather(normed, 'tp', axis=0, tiled=True)  15.4 us
    unnamed x48, local copies, waits for them, and re-layouts  12.1 us
    dot_general x1, matrix products, body(): jnp.dot(lax.all_gather(source_normed, 'tp', axis=0, tiled=True), joined_w...  8.86 us
  transfers between devices with their start and end apart: 15, of which 14 were waited for; matrix products, arithmetic and copies ran while one was open for 7% of the time, Pallas kernels for 0%

profile of v1, /device:TPU:0, one launch (start us, length us, event | category | flops | bytes accessed | tf_op | source)
XLA Modules:
  0.0 315.4 jit_solution(6345947291347882894)
XLA Ops:
  6.5 1.4 fusion.31
  7.9 2.1 fusion.33
  10.4 8.8 %all_gather.13 = bf16[128,2048]{1,0:T(8,128)(2,1)S(1)} all-gather(bf16[32,2048]{1,0:T(8,128)(2,1)S(1)} %fusion.65), channel_id=1, replica_groups=mesh['grp'=2,'sp'=4,'tp'=4] {'tp'}, dimensions={0}, use_global_device_ids=true | all-gather | bytes 655360 | tf_op jit(solution)/shard_map/all_gather | solution.py:27
  19.2 2.2 fusion.25
  22.0 1.6 collective-permute-start
  23.6 6.0 %collective-permute-done = bf16[128,512]{1,0:T(8,128)(2,1)S(1)} collective-permute-done((bf16[128,512]{1,0:T(8,128)(2,1)S(1)}, bf16[128,512]{1,0:T(8,128)(2,1)S(1)}, u32[]{:S(2)}, u32[]{:S(2)}) %collective-permute-start) | collective-permute-done | bytes 131104 | tf_op jit(solution)/shard_map/ppermute | solution.py:37
  29.6 0.7 copy-done.11
  30.2 6.8 %collective-permute-done.1 = bf16[128,512]{1,0:T(8,128)(2,1)S(1)} collective-permute-done((bf16[128,512]{1,0:T(8,128)(2,1)S(1)}, bf16[128,512]{1,0:T(8,128)(2,1)S(1)}, u32[]{:S(2)}, u32[]{:S(2)}) %collective-permute-start.1) | collective-permute-done | bytes 131104 | tf_op jit(solution)/shard_map/ppermute | solution.py:37
  37.0 5.0 %slice_bitcast_fusion.2 = (bf16[2048,512]{1,0:T(8,128)(2,1)}, bf16[2048,512]{1,0:T(8,128)(2,1)}, bf16[2048,512]{1,0:T(8,128)(2,1)}, bf16[2048,512]{1,0:T(8,128)(2,1)}) fusion(bf16[2,2048,512]{2,1,0:T(8,128)(2,1)S(1)} %copy-done.3, bf16[2,2048,512]{2,1,0:T(8,128)(2,1)} %param.22), kind=kLoop, calls=%fused_computation.26 | loop fusion | bytes 16777216 | tf_op jit(solution)/shard_map/squeeze | solution.py:89
  42.0 1.9 collective-permute-done.2
  43.9 2.2 fusion.52
  46.1 1.0 copy.32
  47.1 8.9 %fusion.8 = bf16[512,2048]{1,0:T(8,128)(2,1)S(1)} fusion(bf16[512,2048]{1,0:T(8,128)(2,1)} %all-gather.2.cloned.1.call-done, bf16[2048,512]{1,0:T(8,128)(2,1)} %get-tuple-element.12, bf16[2048,512]{1,0:T(8,128)(2,1)} %get-tuple-element.23, bf16[2048,512]{1,0:T(8,128)(2,1)} %get-tuple-element.11, bf16[2048,512]{1,0:T(8,128)(2,1)} %get-tuple-element.24), kind=kOutput, calls=%fused_computation.8 | convolution fusion | flops 4329570304 | bytes 12582912 | tf_op jit(solution)/shard_map/dot_general | solution.py:91
  56.0 1.3 fusion.73
  57.4 2.1 copy.46
  59.4 2.8 multiply_reduce_fusion.1
  62.3 10.4 %pmax.14 = f32[2,512]{1,0:T(2,128)S(1)} all-reduce(f32[2,512]{1,0:T(2,128)S(1)} %get-tuple-element.19), channel_id=1, replica_groups=mesh['grp'=2,'sp'=4,'tp'=4] {'sp'}, use_global_device_ids=true, to_apply=%region_3.5 | all-reduce | flops 1024 | bytes 8192 | tf_op jit(solution)/shard_map/pmax | solution.py:46
  72.7 2.0 fusion.21
  74.6 0.8 copy.50
  75.5 2.9 convolution_convert_fusion.4
  78.4 2.1 copy.56
  80.6 12.3 %reduce-scatter.24.cloned.1.call-done = bf16[128,2]{1,0:T(8,128)(2,1)} async-done(((bf16[512,2]{1,0:T(8,128)(2,1)}), bf16[128,2]{1,0:T(8,128)(2,1)}) %reduce-scatter.24.cloned.1.call-update) | async-done | bytes 528
  92.9 0.8 copy.51
  93.7 21.5 %reduce-scatter.22.cloned.1.call-done = bf16[128,512]{1,0:T(8,128)(2,1)} async-done(((bf16[512,512]{1,0:T(8,128)(2,1)}), bf16[128,512]{1,0:T(8,128)(2,1)}) %reduce-scatter.22.cloned.1.call-update) | async-done | bytes 131088
  115.2 1.0 copy.57
  116.3 2.9 convolution_convert_fusion.2
  119.2 20.0 %reduce-scatter.16.cloned.1.call-done = bf16[32,2048]{1,0:T(8,128)(2,1)} async-done(((bf16[128,2048]{1,0:T(8,128)(2,1)}), bf16[32,2048]{1,0:T(8,128)(2,1)}) %reduce-scatter.16.cloned.1.call-update) | async-done | bytes 131088 | tf_op jit(solution)/shard_map/reduce_scatter | solution.py:61
  139.2 1.1 multiply_reduce_fusion.4
  140.3 1.1 multiply_convert_fusion.2
  141.3 6.6 %all_gather.14 = bf16[128,2048]{1,0:T(8,128)(2,1)S(1)} all-gather(bf16[32,2048]{1,0:T(8,128)(2,1)S(1)} %multiply_convert_fusion.2), channel_id=1, replica_groups=mesh['grp'=2,'sp'=4,'tp'=4] {'tp'}, dimensions={0}, use_global_device_ids=true | all-gather | bytes 655360 | tf_op jit(solution)/shard_map/all_gather | solution.py:27
  147.9 2.0 fusion.28
  150.0 0.6 copy-done.13
  150.6 1.5 collective-permute-start.3
  152.2 6.0 %collective-permute-done.3 = bf16[128,512]{1,0:T(8,128)(2,1)S(1)} collective-permute-done((bf16[128,512]{1,0:T(8,128)(2,1)S(1)}, bf16[128,512]{1,0:T(8,128)(2,1)S(1)}, u32[]{:S(2)}, u32[]{:S(2)}) %collective-permute-start.3) | collective-permute-done | bytes 131104 | tf_op jit(solution)/shard_map/ppermute | solution.py:37
  158.2 0.7 copy-done.14
  158.8 6.9 %collective-permute-done.4 = bf16[128,512]{1,0:T(8,128)(2,1)} collective-permute-done((bf16[128,512]{1,0:T(8,128)(2,1)S(1)}, bf16[128,512]{1,0:T(8,128)(2,1)}, u32[]{:S(2)}, u32[]{:S(2)}) %collective-permute-start.4) | collective-permute-done | bytes 131104 | tf_op jit(solution)/shard_map/ppermute | solution.py:37
  165.7 1.0 copy.47
  166.7 6.1 %collective-permute-done.5 = bf16[128,512]{1,0:T(8,128)(2,1)} collective-permute-done((bf16[128,512]{1,0:T(8,128)(2,1)}, bf16[128,512]{1,0:T(8,128)(2,1)}, u32[]{:S(2)}, u32[]{:S(2)}) %collective-permute-start.5) | collective-permute-done | bytes 131104 | tf_op jit(solution)/shard_map/ppermute | solution.py:37
  172.8 2.2 fusion.45
  175.0 1.0 copy.37
  176.0 3.0 multiply_reduce_fusion
  179.1 8.3 %pmax.15 = f32[2,512]{1,0:T(2,128)S(1)} all-reduce(f32[2,512]{1,0:T(2,128)S(1)} %get-tuple-element.21), channel_id=1, replica_groups=mesh['grp'=2,'sp'=4,'tp'=4] {'sp'}, use_global_device_ids=true, to_apply=%region_10.12 | all-reduce | flops 1024 | bytes 8192 | tf_op jit(solution)/shard_map/pmax | solution.py:46
  187.4 2.0 fusion.23
  189.4 0.8 copy.54
  190.3 2.9 convolution_convert_fusion.3
  193.2 2.0 copy.58
  195.3 13.8 %reduce-scatter.28.cloned.1.call-done = bf16[128,2]{1,0:T(8,128)(2,1)} async-done(((bf16[512,2]{1,0:T(8,128)(2,1)}), bf16[128,2]{1,0:T(8,128)(2,1)}) %reduce-scatter.28.cloned.1.call-update) | async-done | bytes 528
  209.1 0.8 copy.55
  209.9 21.3 %reduce-scatter.26.cloned.1.call-done = bf16[128,512]{1,0:T(8,128)(2,1)} async-done(((bf16[512,512]{1,0:T(8,128)(2,1)}), bf16[128,512]{1,0:T(8,128)(2,1)}) %reduce-scatter.26.cloned.1.call-update) | async-done | bytes 131088
  231.3 1.0 copy.59
  232.3 2.9 convolution_convert_fusion.1
  235.3 19.9 %reduce-scatter.18.cloned.1.call-done = bf16[32,2048]{1,0:T(8,128)(2,1)} async-done(((bf16[128,2048]{1,0:T(8,128)(2,1)}), bf16[32,2048]{1,0:T(8,128)(2,1)}) %reduce-scatter.18.cloned.1.call-update) | async-done | bytes 131088 | tf_op jit(solution)/shard_map/reduce_scatter | solution.py:61
  255.2 1.1 multiply_reduce_fusion.3
  256.3 1.0 multiply_convert_fusion.1
  257.3 6.7 %all_gather.15 = bf16[128,2048]{1,0:T(8,128)(2,1)S(1)} all-gather(bf16[32,2048]{1,0:T(8,128)(2,1)S(1)} %multiply_convert_fusion.1), channel_id=1, replica_groups=mesh['grp'=2,'sp'=4,'tp'=4] {'tp'}, dimensions={0}, use_global_device_ids=true | all-gather | bytes 655360 | tf_op jit(solution)/shard_map/all_gather | solution.py:109
  264.1 2.7 convolution_convert_fusion.5
  266.8 0.9 convolution_convert_fusion.6
  267.9 3.4 %collective-permute-start.6 = (bf16[2,1408]{0,1:T(8,128)(2,1)S(1)}, bf16[2,1408]{0,1:T(8,128)(2,1)S(1)}, u32[]{:S(2)}, u32[]{:S(2)}) collective-permute-start(bf16[2,1408]{0,1:T(8,128)(2,1)S(1)} %pad_maximum_fusion), channel_id=1, source_target_pairs={{0,4},{4,8},{8,12},{1,5},{5,9},{9,13},{2,6},{6,10},{10,14},{3,7},{... | collective-permute-start | bytes 16904 | tf_op jit(solution)/shard_map/ppermute | solution.py:13
  271.5 8.0 %collective-permute-done.6 = bf16[2,1408]{0,1:T(8,128)(2,1)S(1)} collective-permute-done((bf16[2,1408]{0,1:T(8,128)(2,1)S(1)}, bf16[2,1408]{0,1:T(8,128)(2,1)S(1)}, u32[]{:S(2)}, u32[]{:S(2)}) %collective-permute-start.6) | collective-permute-done | bytes 5664 | tf_op jit(solution)/shard_map/ppermute | solution.py:13
  279.8 1.1 fusion.40
  280.9 1.4 convolution_convert_fusion
  282.4 23.4 %reduce-scatter.20.cloned.1.call-done = bf16[32,2048]{1,0:T(8,128)(2,1)} async-done(((bf16[128,2048]{1,0:T(8,128)(2,1)}), bf16[32,2048]{1,0:T(8,128)(2,1)}) %reduce-scatter.20.cloned.1.call-update) | async-done | bytes 131088 | tf_op jit(solution)/shard_map/reduce_scatter | solution.py:121
  305.8 1.1 multiply_reduce_fusion.2
  306.9 1.7 multiply_convert_fusion
  (73 shorter events, 2.1 us)
Async XLA Ops:
  6.5 274.4 %copy-start = (bf16[704,2048]{1,0:T(8,128)(2,1)S(1)}, bf16[704,2048]{1,0:T(8,128)(2,1)}, u32[]{:S(2)}) copy-start(bf16[704,2048]{1,0:T(8,128)(2,1)} %param.30) | copy-start | bytes 8650756
  6.5 3.5 %copy-start.1 = (bf16[32,2048]{1,0:T(8,128)(2,1)S(1)}, bf16[32,2048]{1,0:T(8,128)(2,1)}, u32[]{:S(2)}) copy-start(bf16[32,2048]{1,0:T(8,128)(2,1)} %param.18) | copy-start | bytes 393220
  6.5 3.7 %copy-start.15 = (f32[2,2048]{1,0:T(2,128)S(1)}, f32[2,2048]{1,0:T(2,128)}, u32[]{:S(2)}) copy-start(f32[2,2048]{1,0:T(2,128)} %param.20) | copy-start | bytes 49156
  6.5 40.6 %all-gather.2.cloned.1.call-start = ((), (), s32[]{:S(2)}) async-start(), calls=%async_computation.7 | async-start | bytes 2621440 | tf_op jit(solution)/shard_map/all_gather | solution.py:92
  10.0 82.9 %reduce-scatter.24.cloned.1.call-start = ((), (), s32[]{:S(2)}) async-start(), calls=%async_computation.12 | async-start | bytes 163840
  10.3 26.7 %copy-start.3 = (bf16[2,2048,512]{2,1,0:T(8,128)(2,1)S(1)}, bf16[2,2048,512]{2,1,0:T(8,128)(2,1)}, u32[]{:S(2)}) copy-start(bf16[2,2048,512]{2,1,0:T(8,128)(2,1)} %param.23) | copy-start | bytes 12582916
  21.3 0.6 copy-start.10
  22.0 7.6 %collective-permute-start = (bf16[128,512]{1,0:T(8,128)(2,1)S(1)}, bf16[128,512]{1,0:T(8,128)(2,1)S(1)}, u32[]{:S(2)}, u32[]{:S(2)}) collective-permute-start(bf16[128,512]{1,0:T(8,128)(2,1)S(1)} %fusion.25), channel_id=1, source_target_pairs={{0,4},{4,8},{8,12},{12,0},{1,5},{5,9},{9,13},{13,1},{2,6},{6,10},{... | collective-permute-start | bytes 393224 | tf_op jit(solution)/shard_map/ppermute | solution.py:37
  29.6 0.7 copy-start.11
  30.2 6.8 %collective-permute-start.1 = (bf16[128,512]{1,0:T(8,128)(2,1)S(1)}, bf16[128,512]{1,0:T(8,128)(2,1)S(1)}, u32[]{:S(2)}, u32[]{:S(2)}) collective-permute-start(bf16[128,512]{1,0:T(8,128)(2,1)S(1)} %collective-permute-done), channel_id=1, source_target_pairs={{0,4},{4,8},{8,12},{12,0},{1,5},{5,9},{9,13},{13,1},{2,6},{6,10},{... | collective-permute-start | bytes 393224 | tf_op jit(solution)/shard_map/ppermute | solution.py:37
  37.0 5.0 %copy-start.12 = (bf16[128,512]{1,0:T(8,128)(2,1)}, bf16[128,512]{1,0:T(8,128)(2,1)S(1)}, u32[]{:S(2)}) copy-start(bf16[128,512]{1,0:T(8,128)(2,1)S(1)} %collective-permute-done.1) | copy-start | bytes 393220
  37.0 6.9 %collective-permute-start.2 = (bf16[128,512]{1,0:T(8,128)(2,1)S(1)}, bf16[128,512]{1,0:T(8,128)(2,1)}, u32[]{:S(2)}, u32[]{:S(2)}) collective-permute-start(bf16[128,512]{1,0:T(8,128)(2,1)S(1)} %collective-permute-done.1), channel_id=1, source_target_pairs={{0,4},{4,8},{8,12},{12,0},{1,5},{5,9},{9,13},{13,1},{2,6},{6,10},{... | collective-permute-start | bytes 393224 | tf_op jit(solution)/shard_map/ppermute | solution.py:37
  56.0 3.4 %copy-start.7 = (bf16[512,512]{0,1:T(8,128)(2,1)S(1)}, bf16[512,512]{0,1:T(8,128)(2,1)}, u32[]{:S(2)}) copy-start(bf16[512,512]{0,1:T(8,128)(2,1)} %copy.32) | copy-start | bytes 1572868
  62.3 13.2 %copy-start.8 = (bf16[512,512]{0,1:T(8,128)(2,1)S(1)}, bf16[512,512]{0,1:T(8,128)(2,1)}, u32[]{:S(2)}) copy-start(bf16[512,512]{0,1:T(8,128)(2,1)} %copy.46) | copy-start | bytes 1572868
  75.5 39.7 %reduce-scatter.22.cloned.1.call-start = ((), (), s32[]{:S(2)}) async-start(), calls=%async_computation.11 | async-start | bytes 655360
  80.5 58.7 %reduce-scatter.16.cloned.1.call-start = ((), (), s32[]{:S(2)}) async-start(), calls=%async_computation.8 | async-start | bytes 655360 | tf_op jit(solution)/shard_map/reduce_scatter | solution.py:61
  119.1 90.0 %reduce-scatter.28.cloned.1.call-start = ((), (), s32[]{:S(2)}) async-start(), calls=%async_computation.14 | async-start | bytes 163840
  140.3 25.4 %copy-start.9 = (bf16[512,512]{1,0:T(8,128)(2,1)S(1)}, bf16[512,512]{1,0:T(8,128)(2,1)}, u32[]{:S(2)}) copy-start(bf16[512,512]{1,0:T(8,128)(2,1)} %get-tuple-element.14) | copy-start | bytes 1572868
  150.0 0.7 copy-start.13
  150.6 7.5 %collective-permute-start.3 = (bf16[128,512]{1,0:T(8,128)(2,1)S(1)}, bf16[128,512]{1,0:T(8,128)(2,1)S(1)}, u32[]{:S(2)}, u32[]{:S(2)}) collective-permute-start(bf16[128,512]{1,0:T(8,128)(2,1)S(1)} %fusion.28), channel_id=1, source_target_pairs={{0,4},{4,8},{8,12},{12,0},{1,5},{5,9},{9,13},{13,1},{2,6},{6,10},{... | collective-permute-start | bytes 393224 | tf_op jit(solution)/shard_map/ppermute | solution.py:37
  158.2 0.7 copy-start.14
  158.8 6.9 %collective-permute-start.4 = (bf16[128,512]{1,0:T(8,128)(2,1)S(1)}, bf16[128,512]{1,0:T(8,128)(2,1)}, u32[]{:S(2)}, u32[]{:S(2)}) collective-permute-start(bf16[128,512]{1,0:T(8,128)(2,1)S(1)} %collective-permute-done.3), channel_id=1, source_target_pairs={{0,4},{4,8},{8,12},{12,0},{1,5},{5,9},{9,13},{13,1},{2,6},{6,10},{... | collective-permute-start | bytes 393224 | tf_op jit(solution)/shard_map/ppermute | solution.py:37
  165.7 7.1 %collective-permute-start.5 = (bf16[128,512]{1,0:T(8,128)(2,1)}, bf16[128,512]{1,0:T(8,128)(2,1)}, u32[]{:S(2)}, u32[]{:S(2)}) collective-permute-start(bf16[128,512]{1,0:T(8,128)(2,1)} %collective-permute-done.4), channel_id=1, source_target_pairs={{0,4},{4,8},{8,12},{12,0},{1,5},{5,9},{9,13},{13,1},{2,6},{6,10},{... | collective-permute-start | bytes 393224 | tf_op jit(solution)/shard_map/ppermute | solution.py:37
  176.0 14.2 %copy-start.6 = (bf16[512,512]{0,1:T(8,128)(2,1)S(1)}, bf16[512,512]{0,1:T(8,128)(2,1)}, u32[]{:S(2)}) copy-start(bf16[512,512]{0,1:T(8,128)(2,1)} %copy.47) | copy-start | bytes 1572868
  190.2 41.0 %reduce-scatter.26.cloned.1.call-start = ((), (), s32[]{:S(2)}) async-start(), calls=%async_computation.13 | async-start | bytes 655360
  195.2 60.0 %copy-start.2 = (bf16[32,2048]{1,0:T(8,128)(2,1)S(1)}, bf16[32,2048]{1,0:T(8,128)(2,1)}, u32[]{:S(2)}) copy-start(bf16[32,2048]{1,0:T(8,128)(2,1)} %reduce-scatter.16.cloned.1.call-done) | copy-start | bytes 393220
  195.3 59.9 %reduce-scatter.18.cloned.1.call-start = ((), (), s32[]{:S(2)}) async-start(), calls=%async_computation.9 | async-start | bytes 655360 | tf_op jit(solution)/shard_map/reduce_scatter | solution.py:61
  209.9 46.4 %copy-start.18 = (f32[2048]{0:T(1024)S(1)}, f32[2048]{0:T(1024)}, u32[]{:S(2)}) copy-start(f32[2048]{0:T(1024)} %param.25) | copy-start | bytes 24580
  235.2 70.6 %reduce-scatter.20.cloned.1.call-start = ((), (), s32[]{:S(2)}) async-start(), calls=%async_computation.10 | async-start | bytes 655360 | tf_op jit(solution)/shard_map/reduce_scatter | solution.py:121
  257.3 9.5 %copy-start.4 = (bf16[2048,704]{0,1:T(8,128)(2,1)S(1)}, bf16[2048,704]{0,1:T(8,128)(2,1)}, u32[]{:S(2)}) copy-start(bf16[2048,704]{0,1:T(8,128)(2,1)} %param.26) | copy-start | bytes 8650756
  266.8 4.5 %copy-start.16 = (f32[3,704]{1,0:T(4,128)S(1)}, f32[3,704]{1,0:T(4,128)}, u32[]{:S(2)}) copy-start(f32[3,704]{1,0:T(4,128)} %param.29) | copy-start | bytes 25348
  266.8 4.5 %copy-start.17 = (f32[3,704]{1,0:T(4,128)S(1)}, f32[3,704]{1,0:T(4,128)}, u32[]{:S(2)}) copy-start(f32[3,704]{1,0:T(4,128)} %param.28) | copy-start | bytes 25348
  267.9 11.6 %collective-permute-start.6 = (bf16[2,1408]{0,1:T(8,128)(2,1)S(1)}, bf16[2,1408]{0,1:T(8,128)(2,1)S(1)}, u32[]{:S(2)}, u32[]{:S(2)}) collective-permute-start(bf16[2,1408]{0,1:T(8,128)(2,1)S(1)} %pad_maximum_fusion), channel_id=1, source_target_pairs={{0,4},{4,8},{8,12},{1,5},{5,9},{9,13},{2,6},{6,10},{10,14},{3,7},{... | collective-permute-start | bytes 16904 | tf_op jit(solution)/shard_map/ppermute | solution.py:13
  280.9 24.9 %copy-start.5 = (bf16[32,2048]{1,0:T(8,128)(2,1)S(1)}, bf16[32,2048]{1,0:T(8,128)(2,1)}, u32[]{:S(2)}) copy-start(bf16[32,2048]{1,0:T(8,128)(2,1)} %reduce-scatter.18.cloned.1.call-done) | copy-start | bytes 393220
  280.9 26.0 %copy-start.19 = (f32[2048]{0:T(1024)S(1)}, f32[2048]{0:T(1024)}, u32[]{:S(2)}) copy-start(f32[2048]{0:T(1024)} %param.31) | copy-start | bytes 24580
Sparse Core Ops, SparseCore 0:
  10.1 25.2 all-gather.1
  75.6 17.2 reduce-scatter.23
  95.2 19.9 reduce-scatter.21
  119.3 19.9 reduce-scatter.15
  190.3 18.7 reduce-scatter.27
  211.2 19.9 reduce-scatter.25
  235.3 19.8 reduce-scatter.17
  282.5 23.2 reduce-scatter.19
